TPU v7x, 256 devices: a whole 4x4x8 slice. The times are simulated.
256 devices in a mesh: row: 32 (over z, x), col: 8 (over y, core).
Axes of the slice: x: 4, y: 4, z: 8, core: 2. Of those that a mesh axis runs over, the one named last changes fastest.
Arguments:
- tokens: bfloat16 [2, 32768, 2048], P(None, ('row', 'col')), may hold values from -6 to 6
- norm_gain: float32 [2048], replicated, may hold values from 0.1 to 1.9
- mix_weight: bfloat16 [2048, 1024], replicated, may hold values from -0.125 to 0.125
- gate_weight: bfloat16 [2048, 2048], replicated, may hold values from -0.125 to 0.125
- out_weight: bfloat16 [1024, 2048], replicated, may hold values from -0.1875 to 0.1875
Outputs:
- gated: bfloat16 [2, 32768, 2048], P(None, ('row', 'col'))
All inputs are finite; a program needn't handle non-finite values.
Results may differ from a plain program's by a relative error of at most 0.017.
Values may be sent and summed in bfloat16 or wider, within the bound.
No kernel may reach another device: no remote copies, remote signals or barrier semaphores. Data moves between devices by JAX's collectives and lax.ppermute only.
A program may use at most 128 MiB of HBM per device.

v0:
```python
import math
import jax
import jax.numpy as jnp
from jax import lax
from jax.sharding import Mesh
from jax.sharding import PartitionSpec as P

GROUP_DIM = 128
LEN1 = 128
ROW = ("row_0", "row_1")
ROW_COL = ("row_0", "row_1", "col")


def cut_along(value, dim, peers):
    before, after = (value.shape[:dim], value.shape[dim + 1 :])
    return jnp.moveaxis(value.reshape(*before, peers, -1, *after), dim, 0)


def laid_out(parts, dim):
    lengths = list(parts.shape[1:])
    lengths[dim] *= parts.shape[0]
    return jnp.moveaxis(parts, 0, dim).reshape(lengths)


def exchange_in_order(parts, axes, order):
    inside = parts.shape[1:]
    whole = parts.reshape(*(lax.axis_size(a) for a in axes), *inside)
    for k in order:
        whole = lax.all_to_all(whole, axes[k], k, k, tiled=True)
    return whole.reshape(-1, *inside)


def one_axis_at_a_time(value, axes, order, split_dim, concat_dim):
    parts = cut_along(value, split_dim, lax.axis_size(axes))
    return laid_out(exchange_in_order(parts, axes, order), concat_dim)


def tables(length, factor):
    indices = jnp.arange(length, dtype=jnp.int32)
    products = indices[:, None] * indices[None, :] % length
    angles = products.astype(jnp.float32) * (2.0 * math.pi / length)
    return (jnp.cos(angles) * factor, jnp.sin(angles) * factor)


def length_transform(values, first_span):
    item_count, span_total, column_count = values.shape
    second_span = span_total // first_span
    cos_first, sin_first = tables(first_span, span_total ** (-0.5))
    cos_second, sin_second = tables(second_span, 1.0)
    row_index = jnp.arange(first_span, dtype=jnp.int32)[:, None]
    col_index = jnp.arange(second_span, dtype=jnp.int32)[None, :]
    twist_angle = (row_index * col_index % span_total).astype(jnp.float32) * (
        2.0 * math.pi / span_total
    )
    twist_cos = jnp.cos(twist_angle)[None, :, :, None]
    twist_sin = jnp.sin(twist_angle)[None, :, :, None]
    arranged = values.reshape(item_count, first_span, second_span, column_count)
    part_real = jnp.einsum("ka,sabc->skbc", cos_first, arranged)
    part_imaginary = -jnp.einsum("ka,sabc->skbc", sin_first, arranged)
    turned_real = part_real * twist_cos + part_imaginary * twist_sin
    turned_imaginary = part_imaginary * twist_cos - part_real * twist_sin
    real_part = jnp.einsum("skbc,bm->smkc", turned_real, cos_second) + jnp.einsum(
        "skbc,bm->smkc", turned_imaginary, sin_second
    )
    imaginary = jnp.einsum("skbc,bm->smkc", turned_imaginary, cos_second) - jnp.einsum(
        "skbc,bm->smkc", turned_real, sin_second
    )
    return (
        real_part.reshape(item_count, span_total, column_count),
        imaginary.reshape(item_count, span_total, column_count),
    )


def local(tokens, norm_gain, mix_weight, gate_weight, out_weight):
    widened = tokens.astype(jnp.float32)
    inverse_rms = lax.rsqrt(jnp.mean(widened * widened, axis=-1, keepdims=True) + 1e-06)
    normed = (widened * inverse_rms * norm_gain).astype(jnp.bfloat16)
    mixed_in = jnp.dot(normed, mix_weight, preferred_element_type=jnp.float32).astype(jnp.bfloat16)
    half_dim = GROUP_DIM // 2
    cos_group, sin_group = tables(GROUP_DIM, GROUP_DIM ** (-0.5))
    left_table = cos_group[:, :half_dim]
    right_table = jnp.concatenate(
        [cos_group[:, half_dim : half_dim + 1], sin_group[:, 1:half_dim]], axis=1
    )
    incoming = lax.all_to_all(mixed_in, "col", split_axis=2, concat_axis=1, tiled=True)
    item_count = incoming.shape[0]
    row_count = incoming.shape[1]
    grouped = incoming.astype(jnp.float32).reshape(item_count, row_count, -1, GROUP_DIM)
    left_part = jnp.einsum("srgj,jk->srgk", grouped, left_table)
    right_part = jnp.einsum("srgj,jk->srgk", grouped, right_table)
    spectra = jnp.stack(
        [
            left_part.reshape(item_count, row_count, -1),
            right_part.reshape(item_count, row_count, -1),
        ],
        axis=2,
    )
    gate_value = jax.nn.sigmoid(jnp.dot(normed, gate_weight, preferred_element_type=jnp.float32))
    seq_count, block_rows = (spectra.shape[0], spectra.shape[1])
    pair_width = spectra.shape[3] // lax.axis_size(ROW)
    flat_index = lax.axis_index(ROW) * pair_width + jnp.arange(pair_width, dtype=jnp.int32)
    lone_pair = flat_index % half_dim == 0
    stacked = lax.all_to_all(
        spectra.astype(jnp.bfloat16), ROW, split_axis=3, concat_axis=1, tiled=True
    ).astype(spectra.dtype)
    width_here = stacked.shape[3]
    joined_in = jnp.concatenate([stacked[:, :, 0], stacked[:, :, 1]], axis=2)
    real_part, imaginary = length_transform(joined_in, LEN1)
    sum_pair = real_part[..., :width_here] + imaginary[..., width_here:]
    diff_pair = real_part[..., :width_here] - imaginary[..., width_here:]
    lower_half = jnp.where(lone_pair, real_part[..., :width_here], sum_pair).astype(jnp.bfloat16)
    upper_half = jnp.where(lone_pair, real_part[..., width_here:], diff_pair).astype(jnp.bfloat16)
    both_halves = jnp.stack([lower_half, upper_half], axis=2)
    returned = one_axis_at_a_time(both_halves, ROW, (0, 1), 1, 3)
    lower_half = returned[:, :, 0].reshape(seq_count, block_rows, -1, half_dim)
    upper_half = returned[:, :, 1].reshape(seq_count, block_rows, -1, half_dim)
    spectral = jnp.concatenate(
        [lower_half, upper_half[..., :1], jnp.flip(upper_half[..., 1:], axis=3)], axis=3
    )
    spectral = spectral.reshape(seq_count, block_rows, -1)
    spectral_rows = lax.all_to_all(spectral, "col", split_axis=1, concat_axis=2, tiled=True)
    mapped = jnp.dot(spectral_rows, out_weight, preferred_element_type=jnp.float32)
    return (gate_value * mapped).astype(jnp.bfloat16)


def solution(mesh):
    split = Mesh(mesh.devices.reshape(8, 4, mesh.shape["col"]), ("row_0", "row_1", "col"))
    return jax.shard_map(
        local,
        mesh=split,
        in_specs=(P(None, ROW_COL, None), P(), P(), P(), P()),
        out_specs=P(None, ROW_COL, None),
        check_vma=False,
    )
```

profile of v0, /device:TPU:1, one launch (start us, length us, event | category | flops | bytes accessed | tf_op | source)
XLA Modules:
  0.0 124.7 jit_solution(7634107121673975796)
XLA Ops:
  0.0 1.5 %fusion.24 = f32[2,128]{1,0:T(2,128)S(1)} fusion(bf16[2,128,2048]{2,1,0:T(8,128)(2,1)} %param.5), kind=kLoop, calls=%fused_computation.14 | loop fusion | flops 1572608 | bytes 1049600 | tf_op jit(solution)/shard_map/reduce_sum | solution.py:76
  1.5 3.8 %fusion.30 = bf16[2,128,1024]{2,1,0:T(8,128)(2,1)S(1)} fusion(bf16[2048,1024]{1,0:T(8,128)(2,1)} %param.7, bf16[2,128,2048]{2,1,0:T(8,128)(2,1)} %param.5, f32[2048]{0:T(1024)} %param.6, f32[2,128]{1,0:T(2,128)S(1)} %add_rsqrt_fusion), kind=kOutput, calls=%fused_computation.24 | convolution fusion | flops 1076101120 | bytes 5776384 | tf_op jit(solution)/shard_map/dot_general | solution.py:78
  5.4 1.1 copy.63
  6.5 6.6 %all-to-all-start = ((bf16[2,128,1024]{1,0,2:T(2,128)(2,1)}), bf16[2,128,1024]{1,0,2:T(2,128)(2,1)S(1)}, u32[]{:S(2)}, u32[]{:S(2)}) async-start(bf16[2,128,1024]{1,0,2:T(2,128)(2,1)} %copy.63), calls=%async_computation | async-start | bytes 1048576 | tf_op jit(solution)/shard_map/all_to_all | solution.py:85
  13.6 8.8 %all-to-all-done = bf16[2,128,1024]{1,0,2:T(2,128)(2,1)S(1)} async-done(((bf16[2,128,1024]{1,0,2:T(2,128)(2,1)}), bf16[2,128,1024]{1,0,2:T(2,128)(2,1)S(1)}, u32[]{:S(2)}, u32[]{:S(2)}) %all-to-all-start) | async-done | bytes 524320 | tf_op jit(solution)/shard_map/all_to_all | solution.py:85
  23.6 1.3 %copy.65 = bf16[2,1024,2,64]{1,0,2,3:T(2,128)(2,1)} copy(bf16[2,1024,2,64]{1,3,0,2:T(8,128)(2,1)S(1)} %pad_maximum_fusion.4) | data formatting | bytes 1048576 | tf_op jit(solution)/shard_map/stack | solution.py:91
  24.9 10.5 %all-to-all-start.1 = ((bf16[2,1024,2,64]{1,0,2,3:T(2,128)(2,1)}), bf16[2,1024,2,64]{1,0,2,3:T(2,128)(2,1)S(1)}, u32[]{:S(2)}, u32[]{:S(2)}) async-start(bf16[2,1024,2,64]{1,0,2,3:T(2,128)(2,1)} %copy.65), calls=%async_computation.1 | async-start | bytes 1048576 | tf_op jit(solution)/shard_map/all_to_all | solution.py:103
  36.0 14.9 %all-to-all-done.1 = bf16[2,1024,2,64]{1,0,2,3:T(2,128)(2,1)S(1)} async-done(((bf16[2,1024,2,64]{1,0,2,3:T(2,128)(2,1)}), bf16[2,1024,2,64]{1,0,2,3:T(2,128)(2,1)S(1)}, u32[]{:S(2)}, u32[]{:S(2)}) %all-to-all-start.1) | async-done | bytes 524320 | tf_op jit(solution)/shard_map/all_to_all | solution.py:103
  53.7 1.3 %fusion.48 = f32[256,2,128,4]{2,0,3,1:T(8,128)S(1)} fusion(f32[2,128,256,4]{1,2,3,0:T(8,128)S(1)} %fusion.27, f32[2,128,256,4]{1,2,3,0:T(8,128)S(1)} %convolution_bitcast_fusion, f32[128,256]{0,1:T(8,128)S(1)} %get-tuple-element.9, f32[128,256]{0,1:T(8,128)S(1)} %get-tuple-element.10), kind=kOutput, calls=%fused_computation.52 | convolution fusion | flops 135921664 | bytes 3407872 | tf_op jit(solution)/shard_map/skbc,bm->smkc/dot_general | solution.py:62
  55.0 1.3 %fusion.46 = f32[256,2,128,4]{2,0,3,1:T(8,128)S(1)} fusion(f32[2,128,256,4]{1,2,3,0:T(8,128)S(1)} %convolution_bitcast_fusion, f32[2,128,256,4]{1,2,3,0:T(8,128)S(1)} %fusion.27, f32[128,256]{0,1:T(8,128)S(1)} %get-tuple-element.9, f32[128,256]{0,1:T(8,128)S(1)} %get-tuple-element.10), kind=kOutput, calls=%fused_computation.50 | convolution fusion | flops 135921664 | bytes 3407872 | tf_op jit(solution)/shard_map/skbc,bm->smkc/dot_general | solution.py:65
  56.3 2.3 %fusion.29 = f32[2,256,128,4]{2,1,3,0:T(8,128)} fusion(f32[256,2,128,4]{2,0,3,1:T(8,128)S(1)} %fusion.48, f32[2,128,256,4]{1,2,3,0:T(8,128)S(1)} %convolution_bitcast_fusion, f32[2,128,256,4]{1,2,3,0:T(8,128)S(1)} %fusion.27, f32[128,256]{0,1:T(8,128)S(1)} %get-tuple-element.9, f32[128,256]{0,1:T(8,128)S(1)} %get-tuple-element.10), kind=kOutput, calls=%fused_computation.23 | convolution fusion | flops 136183808 | bytes 4456448 | tf_op jit(solution)/shard_map/skbc,bm->smkc/dot_general | solution.py:62
  58.6 2.7 %reshape.92 = f32[2,32768,4]{1,2,0:T(4,128)} reshape(f32[2,256,128,4]{2,1,3,0:T(8,128)} %fusion.29) | data formatting | bytes 2097152 | tf_op jit(solution)/shard_map/reshape | solution.py:69
  61.3 2.3 %fusion.28 = f32[2,256,128,4]{2,1,3,0:T(8,128)} fusion(f32[256,2,128,4]{2,0,3,1:T(8,128)S(1)} %fusion.46, f32[2,128,256,4]{1,2,3,0:T(8,128)S(1)} %fusion.27, f32[2,128,256,4]{1,2,3,0:T(8,128)S(1)} %convolution_bitcast_fusion, f32[128,256]{0,1:T(8,128)S(1)} %get-tuple-element.9, f32[128,256]{0,1:T(8,128)S(1)} %get-tuple-element.10), kind=kOutput, calls=%fused_computation.21 | convolution fusion | flops 136183808 | bytes 4456448 | tf_op jit(solution)/shard_map/skbc,bm->smkc/dot_general | solution.py:65
  63.5 1.8 %reshape.93 = f32[2,32768,4]{1,2,0:T(4,128)S(1)} reshape(f32[2,256,128,4]{2,1,3,0:T(8,128)} %fusion.28) | data formatting | bytes 2097152 | tf_op jit(solution)/shard_map/reshape | solution.py:70
  65.3 0.8 fusion.37
  67.6 17.5 %all_to_all.52 = bf16[8,4,2,1024,2,2]{3,4,5,1,2,0:T(2,128)(2,1)S(1)} all-to-all(bf16[8,4,2,1024,2,2]{3,4,5,1,2,0:T(2,128)(2,1)S(1)} %copy.76), channel_id=1, replica_groups=mesh['row_0'=8,'row_1'=4,'col'=8] {'row_0'}, dimensions={0} | all-to-all | bytes 1048576 | tf_op jit(solution)/shard_map/all_to_all | solution.py:29
  85.5 10.9 %all_to_all.53 = bf16[8,4,2,1024,2,2]{3,4,5,0,2,1:T(2,128)(2,1)S(1)} all-to-all(bf16[8,4,2,1024,2,2]{3,4,5,0,2,1:T(2,128)(2,1)S(1)} %copy.77), channel_id=1, replica_groups=mesh['row_0'=8,'row_1'=4,'col'=8] {'row_1'}, dimensions={1} | all-to-all | bytes 1048576 | tf_op jit(solution)/shard_map/all_to_all | solution.py:29
  98.5 1.5 %pad_maximum_fusion.1 = bf16[2,1024,1,128]{1,2,3,0:T(2,128)(2,1)S(1)} fusion(bf16[2,1024,1,63]{1,2,3,0:T(2,128)(2,1)S(1)} %rev.4, bf16[2,1024,1,1]{1,2,3,0:T(2,128)(2,1)S(1)} %slice.59, bf16[2,1024,1,64]{1,2,3,0:T(2,128)(2,1)S(1)} %bitcast.112), kind=kLoop, calls=%fused_computation.30 | loop fusion | flops 524288 | bytes 1048576 | tf_op jit(solution)/shard_map/concatenate | solution.py:117
  100.0 0.9 copy.80
  100.9 1.3 %copy.81 = bf16[2,1024,128]{2,0,1:T(2,128)(2,1)} copy(bf16[2,1024,128]{2,1,0:T(8,128)(2,1)S(1)} %bitcast.113) | data formatting | bytes 1048576 | tf_op jit(solution)/shard_map/reshape | solution.py:120
  102.2 8.5 %all-to-all-start.4 = ((bf16[2,1024,128]{2,0,1:T(2,128)(2,1)}), bf16[2,1024,128]{2,0,1:T(2,128)(2,1)S(1)}, u32[]{:S(2)}, u32[]{:S(2)}) async-start(bf16[2,1024,128]{2,0,1:T(2,128)(2,1)} %copy.81), calls=%async_computation.4 | async-start | bytes 1048576 | tf_op jit(solution)/shard_map/all_to_all | solution.py:121
  110.8 6.2 %fusion.21 = f32[2,128,2048]{2,1,0:T(8,128)S(1)} fusion(bf16[2048,2048]{1,0:T(8,128)(2,1)} %param.8, bf16[2,128,2048]{2,1,0:T(8,128)(2,1)} %param.5, f32[2048]{0:T(1024)S(1)} %copy-done.1, f32[2,128]{1,0:T(2,128)S(1)} %add_rsqrt_fusion), kind=kOutput, calls=%fused_computation.13 | convolution fusion | flops 2151153664 | bytes 11543552 | tf_op jit(solution)/shard_map/dot_general | solution.py:98
  117.0 3.2 %all-to-all-done.4 = bf16[2,1024,128]{2,0,1:T(2,128)(2,1)S(1)} async-done(((bf16[2,1024,128]{2,0,1:T(2,128)(2,1)}), bf16[2,1024,128]{2,0,1:T(2,128)(2,1)S(1)}, u32[]{:S(2)}, u32[]{:S(2)}) %all-to-all-start.4) | async-done | bytes 524320 | tf_op jit(solution)/shard_map/all_to_all | solution.py:121
  120.2 4.5 %fusion.18 = bf16[2,128,2048]{2,1,0:T(8,128)(2,1)} fusion(f32[2,128,2048]{2,1,0:T(8,128)S(1)} %fusion.21, bf16[1024,2048]{1,0:T(8,128)(2,1)} %param.9, bf16[2,8,16,8,128]{4,3,2,1,0:T(8,128)(2,1)S(1)} %bitcast.119), kind=kOutput, calls=%fused_computation.12 | convolution fusion | flops 1074790400 | bytes 7864320 | tf_op jit(solution)/shard_map/dot_general | solution.py:122
  (36 shorter events, 9.0 us)
Async XLA Ops:
  6.5 16.0 %all-to-all-start = ((bf16[2,128,1024]{1,0,2:T(2,128)(2,1)}), bf16[2,128,1024]{1,0,2:T(2,128)(2,1)S(1)}, u32[]{:S(2)}, u32[]{:S(2)}) async-start(bf16[2,128,1024]{1,0,2:T(2,128)(2,1)} %copy.63), calls=%async_computation | async-start | bytes 1048576 | tf_op jit(solution)/shard_map/all_to_all | solution.py:85
  24.9 26.0 %all-to-all-start.1 = ((bf16[2,1024,2,64]{1,0,2,3:T(2,128)(2,1)}), bf16[2,1024,2,64]{1,0,2,3:T(2,128)(2,1)S(1)}, u32[]{:S(2)}, u32[]{:S(2)}) async-start(bf16[2,1024,2,64]{1,0,2,3:T(2,128)(2,1)} %copy.65), calls=%async_computation.1 | async-start | bytes 1048576 | tf_op jit(solution)/shard_map/all_to_all | solution.py:103
  63.5 1.8 %copy-start = (f32[2,32768,4]{1,2,0:T(4,128)S(1)}, f32[2,32768,4]{1,2,0:T(4,128)}, u32[]{:S(2)}) copy-start(f32[2,32768,4]{1,2,0:T(4,128)} %reshape.92) | copy-start | bytes 3145732
  100.0 10.8 %copy-start.1 = (f32[2048]{0:T(1024)S(1)}, f32[2048]{0:T(1024)}, u32[]{:S(2)}) copy-start(f32[2048]{0:T(1024)} %param.6) | copy-start | bytes 24580
  102.2 17.9 %all-to-all-start.4 = ((bf16[2,1024,128]{2,0,1:T(2,128)(2,1)}), bf16[2,1024,128]{2,0,1:T(2,128)(2,1)S(1)}, u32[]{:S(2)}, u32[]{:S(2)}) async-start(bf16[2,1024,128]{2,0,1:T(2,128)(2,1)} %copy.81), calls=%async_computation.4 | async-start | bytes 1048576 | tf_op jit(solution)/shard_map/all_to_all | solution.py:121
where the time goes:
time: 125 us
  blocking collectives  28.4 us (23%)
  waiting for transfers between devices  26.9 us (22%)
  starting transfers between devices  25.7 us (21%)
  matrix products  23.3 us (19%)
  local copies, waits for them, and re-layouts  15.2 us (12%)
  other arithmetic  4.97 us (4%)
    all_to_all x2, blocking collectives, exchange_in_order(): whole = lax.all_to_all(whole, axes[k], k, k, tiled=True)  28.4 us
    all_to_all x1, waiting for transfers between devices, local(): lax.all_to_all(spectra.astype(jnp.bfloat16), ROW, split_axis=3, concat_ax...  14.9 us
    all_to_all x1, starting transfers between devices, local(): lax.all_to_all(spectra.astype(jnp.bfloat16), ROW, split_axis=3, concat_ax...  10.5 us
    all_to_all x1, waiting for transfers between devices, local(): lax.all_to_all(mixed_in, 'col', split_axis=2, concat_axis=1, tiled=True)  8.82 us
    all_to_all x1, starting transfers between devices, local(): lax.all_to_all(spectral, 'col', split_axis=1, concat_axis=2, tiled=True)  8.54 us
    all_to_all x1, starting transfers between devices, local(): lax.all_to_all(mixed_in, 'col', split_axis=2, concat_axis=1, tiled=True)  6.6 us
    dot_general x1, matrix products, local(): jnp.dot(normed, gate_weight, preferred_element_type=jnp.float32)  6.2 us
    dot_general x1, matrix products, local(): jnp.dot(spectral_rows, out_weight, preferred_element_type=jnp.float32)  4.48 us
  transfers between devices with their start and end apart: 3, of which 3 were waited for; matrix products, arithmetic and copies ran while one was open for 6% of the time, Pallas kernels for 0%

commit v1 on v0

--- a/solution.py
+++ b/solution.py
@@ -82,7 +82,10 @@
     right_table = jnp.concatenate(
         [cos_group[:, half_dim : half_dim + 1], sin_group[:, 1:half_dim]], axis=1
     )
-    incoming = lax.all_to_all(mixed_in, "col", split_axis=2, concat_axis=1, tiled=True)
+    count = lax.axis_size("col")
+    tiles = jnp.stack(jnp.split(mixed_in, count, axis=2), axis=0)
+    tiles = lax.all_to_all(tiles, "col", split_axis=0, concat_axis=0)
+    incoming = jnp.concatenate(tiles, axis=1)
     item_count = incoming.shape[0]
     row_count = incoming.shape[1]
     grouped = incoming.astype(jnp.float32).reshape(item_count, row_count, -1, GROUP_DIM)

time: 125 us -> 129 us (1.032)
  local copies, waits for them, and re-layouts: 15.2 us -> 18.9 us
    unnamed x4 -> x11, local copies, waits for them, and re-layouts: 0.01 us -> 4.54 us
where the time goes in v1:
time: 129 us; the launch traced here: 128 us
  blocking collectives  28.4 us (22%)
  waiting for transfers between devices  26.9 us (21%)
  starting transfers between devices  25.7 us (20%)
  matrix products  23.3 us (18%)
  local copies, waits for them, and re-layouts  18.9 us (15%)
  other arithmetic  4.97 us (4%)
    all_to_all x2, blocking collectives, exchange_in_order(): whole = lax.all_to_all(whole, axes[k], k, k, tiled=True)  28.4 us
    all_to_all x1, waiting for transfers between devices, local(): lax.all_to_all(spectra.astype(jnp.bfloat16), ROW, split_axis=3, concat_ax...  14.9 us
    all_to_all x1, starting transfers between devices, local(): lax.all_to_all(spectra.astype(jnp.bfloat16), ROW, split_axis=3, concat_ax...  10.6 us
    all_to_all x1, waiting for transfers between devices, local(): tiles = lax.all_to_all(tiles, 'col', split_axis=0, concat_axis=0)  8.82 us
    all_to_all x1, starting transfers between devices, local(): lax.all_to_all(spectral, 'col', split_axis=1, concat_axis=2, tiled=True)  8.54 us
    all_to_all x1, starting transfers between devices, local(): tiles = lax.all_to_all(tiles, 'col', split_axis=0, concat_axis=0)  6.6 us
    dot_general x1, matrix products, local(): jnp.dot(normed, gate_weight, preferred_element_type=jnp.float32)  6.2 us
    unnamed x11, local copies, waits for them, and re-layouts  4.54 us
  transfers between devices with their start and end apart: 3, of which 3 were waited for; matrix products, arithmetic and copies ran while one was open for 6% of the time, Pallas kernels for 0%

profile of v1, /device:TPU:1, one launch (start us, length us, event | category | flops | bytes accessed | tf_op | source)
XLA Modules:
  0.0 128.4 jit_solution(14056710694698260826)
XLA Ops:
  0.0 1.5 %fusion.24 = f32[2,128]{1,0:T(2,128)S(1)} fusion(bf16[2,128,2048]{2,1,0:T(8,128)(2,1)} %param.5), kind=kLoop, calls=%fused_computation.14 | loop fusion | flops 1572608 | bytes 1049600 | tf_op jit(solution)/shard_map/reduce_sum | solution.py:76
  1.5 3.8 %fusion.30 = bf16[2,128,1024]{2,1,0:T(8,128)(2,1)S(1)} fusion(bf16[2048,1024]{1,0:T(8,128)(2,1)} %param.7, bf16[2,128,2048]{2,1,0:T(8,128)(2,1)} %param.5, f32[2048]{0:T(1024)} %param.6, f32[2,128]{1,0:T(2,128)S(1)} %add_rsqrt_fusion), kind=kOutput, calls=%fused_computation.24 | convolution fusion | flops 1076101120 | bytes 5776384 | tf_op jit(solution)/shard_map/dot_general | solution.py:78
  5.4 0.6 fusion.75
  10.5 6.6 %all-to-all-start = ((bf16[8,2,128,128]{3,2,1,0:T(8,128)(2,1)}), bf16[8,2,128,128]{3,2,1,0:T(8,128)(2,1)S(1)}, u32[]{:S(2)}, u32[]{:S(2)}) async-start(bf16[8,2,128,128]{3,2,1,0:T(8,128)(2,1)} %fusion.68), calls=%async_computation | async-start | bytes 1048576 | tf_op jit(solution)/shard_map/all_to_all | solution.py:87
  17.7 8.8 %all-to-all-done = bf16[8,2,128,128]{3,2,1,0:T(8,128)(2,1)S(1)} async-done(((bf16[8,2,128,128]{3,2,1,0:T(8,128)(2,1)}), bf16[8,2,128,128]{3,2,1,0:T(8,128)(2,1)S(1)}, u32[]{:S(2)}, u32[]{:S(2)}) %all-to-all-start) | async-done | bytes 524320 | tf_op jit(solution)/shard_map/all_to_all | solution.py:87
  27.2 1.3 %copy.61 = bf16[2,1024,2,64]{1,0,2,3:T(2,128)(2,1)} copy(bf16[2,1024,2,64]{1,3,0,2:T(8,128)(2,1)S(1)} %pad_maximum_fusion.4) | data formatting | bytes 1048576 | tf_op jit(solution)/shard_map/stack | solution.py:94
  28.6 10.6 %all-to-all-start.1 = ((bf16[2,1024,2,64]{1,0,2,3:T(2,128)(2,1)}), bf16[2,1024,2,64]{1,0,2,3:T(2,128)(2,1)S(1)}, u32[]{:S(2)}, u32[]{:S(2)}) async-start(bf16[2,1024,2,64]{1,0,2,3:T(2,128)(2,1)} %copy.61), calls=%async_computation.1 | async-start | bytes 1048576 | tf_op jit(solution)/shard_map/all_to_all | solution.py:106
  39.7 14.9 %all-to-all-done.1 = bf16[2,1024,2,64]{1,0,2,3:T(2,128)(2,1)S(1)} async-done(((bf16[2,1024,2,64]{1,0,2,3:T(2,128)(2,1)}), bf16[2,1024,2,64]{1,0,2,3:T(2,128)(2,1)S(1)}, u32[]{:S(2)}, u32[]{:S(2)}) %all-to-all-start.1) | async-done | bytes 524320 | tf_op jit(solution)/shard_map/all_to_all | solution.py:106
  57.4 1.3 %fusion.48 = f32[256,2,128,4]{2,0,3,1:T(8,128)S(1)} fusion(f32[2,128,256,4]{1,2,3,0:T(8,128)S(1)} %fusion.27, f32[2,128,256,4]{1,2,3,0:T(8,128)S(1)} %convolution_bitcast_fusion, f32[128,256]{0,1:T(8,128)S(1)} %get-tuple-element.9, f32[128,256]{0,1:T(8,128)S(1)} %get-tuple-element.10), kind=kOutput, calls=%fused_computation.52 | convolution fusion | flops 135921664 | bytes 3407872 | tf_op jit(solution)/shard_map/skbc,bm->smkc/dot_general | solution.py:62
  58.7 1.3 %fusion.46 = f32[256,2,128,4]{2,0,3,1:T(8,128)S(1)} fusion(f32[2,128,256,4]{1,2,3,0:T(8,128)S(1)} %convolution_bitcast_fusion, f32[2,128,256,4]{1,2,3,0:T(8,128)S(1)} %fusion.27, f32[128,256]{0,1:T(8,128)S(1)} %get-tuple-element.9, f32[128,256]{0,1:T(8,128)S(1)} %get-tuple-element.10), kind=kOutput, calls=%fused_computation.50 | convolution fusion | flops 135921664 | bytes 3407872 | tf_op jit(solution)/shard_map/skbc,bm->smkc/dot_general | solution.py:65
  60.0 2.3 %fusion.29 = f32[2,256,128,4]{2,1,3,0:T(8,128)} fusion(f32[256,2,128,4]{2,0,3,1:T(8,128)S(1)} %fusion.48, f32[2,128,256,4]{1,2,3,0:T(8,128)S(1)} %convolution_bitcast_fusion, f32[2,128,256,4]{1,2,3,0:T(8,128)S(1)} %fusion.27, f32[128,256]{0,1:T(8,128)S(1)} %get-tuple-element.9, f32[128,256]{0,1:T(8,128)S(1)} %get-tuple-element.10), kind=kOutput, calls=%fused_computation.23 | convolution fusion | flops 136183808 | bytes 4456448 | tf_op jit(solution)/shard_map/skbc,bm->smkc/dot_general | solution.py:62
  62.3 2.7 %reshape.97 = f32[2,32768,4]{1,2,0:T(4,128)} reshape(f32[2,256,128,4]{2,1,3,0:T(8,128)} %fusion.29) | data formatting | bytes 2097152 | tf_op jit(solution)/shard_map/reshape | solution.py:69
  64.9 2.3 %fusion.28 = f32[2,256,128,4]{2,1,3,0:T(8,128)} fusion(f32[256,2,128,4]{2,0,3,1:T(8,128)S(1)} %fusion.46, f32[2,128,256,4]{1,2,3,0:T(8,128)S(1)} %fusion.27, f32[2,128,256,4]{1,2,3,0:T(8,128)S(1)} %convolution_bitcast_fusion, f32[128,256]{0,1:T(8,128)S(1)} %get-tuple-element.9, f32[128,256]{0,1:T(8,128)S(1)} %get-tuple-element.10), kind=kOutput, calls=%fused_computation.21 | convolution fusion | flops 136183808 | bytes 4456448 | tf_op jit(solution)/shard_map/skbc,bm->smkc/dot_general | solution.py:65
  67.2 1.8 %reshape.98 = f32[2,32768,4]{1,2,0:T(4,128)S(1)} reshape(f32[2,256,128,4]{2,1,3,0:T(8,128)} %fusion.28) | data formatting | bytes 2097152 | tf_op jit(solution)/shard_map/reshape | solution.py:70
  69.0 0.8 fusion.37
  71.3 17.4 %all_to_all.42 = bf16[8,4,2,1024,2,2]{3,4,5,1,2,0:T(2,128)(2,1)S(1)} all-to-all(bf16[8,4,2,1024,2,2]{3,4,5,1,2,0:T(2,128)(2,1)S(1)} %copy.72), channel_id=1, replica_groups=mesh['row_0'=8,'row_1'=4,'col'=8] {'row_0'}, dimensions={0} | all-to-all | bytes 1048576 | tf_op jit(solution)/shard_map/all_to_all | solution.py:29
  89.1 10.9 %all_to_all.43 = bf16[8,4,2,1024,2,2]{3,4,5,0,2,1:T(2,128)(2,1)S(1)} all-to-all(bf16[8,4,2,1024,2,2]{3,4,5,0,2,1:T(2,128)(2,1)S(1)} %copy.73), channel_id=1, replica_groups=mesh['row_0'=8,'row_1'=4,'col'=8] {'row_1'}, dimensions={1} | all-to-all | bytes 1048576 | tf_op jit(solution)/shard_map/all_to_all | solution.py:29
  102.1 1.5 %pad_maximum_fusion.1 = bf16[2,1024,1,128]{1,2,3,0:T(2,128)(2,1)S(1)} fusion(bf16[2,1024,1,63]{1,2,3,0:T(2,128)(2,1)S(1)} %rev.4, bf16[2,1024,1,1]{1,2,3,0:T(2,128)(2,1)S(1)} %slice.59, bf16[2,1024,1,64]{1,2,3,0:T(2,128)(2,1)S(1)} %bitcast.142), kind=kLoop, calls=%fused_computation.30 | loop fusion | flops 524288 | bytes 1048576 | tf_op jit(solution)/shard_map/concatenate | solution.py:120
  103.7 0.9 copy.76
  104.5 1.3 %copy.77 = bf16[2,1024,128]{2,0,1:T(2,128)(2,1)} copy(bf16[2,1024,128]{2,1,0:T(8,128)(2,1)S(1)} %bitcast.143) | data formatting | bytes 1048576 | tf_op jit(solution)/shard_map/reshape | solution.py:123
  105.9 8.5 %all-to-all-start.4 = ((bf16[2,1024,128]{2,0,1:T(2,128)(2,1)}), bf16[2,1024,128]{2,0,1:T(2,128)(2,1)S(1)}, u32[]{:S(2)}, u32[]{:S(2)}) async-start(bf16[2,1024,128]{2,0,1:T(2,128)(2,1)} %copy.77), calls=%async_computation.4 | async-start | bytes 1048576 | tf_op jit(solution)/shard_map/all_to_all | solution.py:124
  114.4 6.2 %fusion.21 = f32[2,128,2048]{2,1,0:T(8,128)S(1)} fusion(bf16[2048,2048]{1,0:T(8,128)(2,1)} %param.8, bf16[2,128,2048]{2,1,0:T(8,128)(2,1)} %param.5, f32[2048]{0:T(1024)S(1)} %copy-done.1, f32[2,128]{1,0:T(2,128)S(1)} %add_rsqrt_fusion), kind=kOutput, calls=%fused_computation.13 | convolution fusion | flops 2151153664 | bytes 11543552 | tf_op jit(solution)/shard_map/dot_general | solution.py:101
  120.6 3.2 %all-to-all-done.4 = bf16[2,1024,128]{2,0,1:T(2,128)(2,1)S(1)} async-done(((bf16[2,1024,128]{2,0,1:T(2,128)(2,1)}), bf16[2,1024,128]{2,0,1:T(2,128)(2,1)S(1)}, u32[]{:S(2)}, u32[]{:S(2)}) %all-to-all-start.4) | async-done | bytes 524320 | tf_op jit(solution)/shard_map/all_to_all | solution.py:124
  123.9 4.5 %fusion.18 = bf16[2,128,2048]{2,1,0:T(8,128)(2,1)} fusion(f32[2,128,2048]{2,1,0:T(8,128)S(1)} %fusion.21, bf16[1024,2048]{1,0:T(8,128)(2,1)} %param.9, bf16[2,8,16,8,128]{4,3,2,1,0:T(8,128)(2,1)S(1)} %bitcast.149), kind=kOutput, calls=%fused_computation.12 | convolution fusion | flops 1074790400 | bytes 7864320 | tf_op jit(solution)/shard_map/dot_general | solution.py:125
  (43 shorter events, 13.1 us)
Async XLA Ops:
  10.5 16.0 %all-to-all-start = ((bf16[8,2,128,128]{3,2,1,0:T(8,128)(2,1)}), bf16[8,2,128,128]{3,2,1,0:T(8,128)(2,1)S(1)}, u32[]{:S(2)}, u32[]{:S(2)}) async-start(bf16[8,2,128,128]{3,2,1,0:T(8,128)(2,1)} %fusion.68), calls=%async_computation | async-start | bytes 1048576 | tf_op jit(solution)/shard_map/all_to_all | solution.py:87
  28.6 26.0 %all-to-all-start.1 = ((bf16[2,1024,2,64]{1,0,2,3:T(2,128)(2,1)}), bf16[2,1024,2,64]{1,0,2,3:T(2,128)(2,1)S(1)}, u32[]{:S(2)}, u32[]{:S(2)}) async-start(bf16[2,1024,2,64]{1,0,2,3:T(2,128)(2,1)} %copy.61), calls=%async_computation.1 | async-start | bytes 1048576 | tf_op jit(solution)/shard_map/all_to_all | solution.py:106
  67.2 1.8 %copy-start = (f32[2,32768,4]{1,2,0:T(4,128)S(1)}, f32[2,32768,4]{1,2,0:T(4,128)}, u32[]{:S(2)}) copy-start(f32[2,32768,4]{1,2,0:T(4,128)} %reshape.97) | copy-start | bytes 3145732
  103.7 10.8 %copy-start.1 = (f32[2048]{0:T(1024)S(1)}, f32[2048]{0:T(1024)}, u32[]{:S(2)}) copy-start(f32[2048]{0:T(1024)} %param.6) | copy-start | bytes 24580
  105.9 17.9 %all-to-all-start.4 = ((bf16[2,1024,128]{2,0,1:T(2,128)(2,1)}), bf16[2,1024,128]{2,0,1:T(2,128)(2,1)S(1)}, u32[]{:S(2)}, u32[]{:S(2)}) async-start(bf16[2,1024,128]{2,0,1:T(2,128)(2,1)} %copy.77), calls=%async_computation.4 | async-start | bytes 1048576 | tf_op jit(solution)/shard_map/all_to_all | solution.py:124
